TPU v7x, 256 devices: a 4x2x16 block of a 4x16x16 slice. The times are simulated.
256 devices in a mesh: grp: 2 (over y), fs: 16 (over z), tp: 8 (over x, core).
Axes of the slice: x: 4, y: 2, z: 16, core: 2. Of those that a mesh axis runs over, the one named last changes fastest.
The devices are a block of a 4x16x16 slice.
Arguments:
- tokens: bfloat16 [32768, 2048], P(('grp', 'fs')), parts along dimension 0, may hold values from -1300 to 1300
- norm_gain: bfloat16 [2048], replicated, may hold values from 0.099609375 to 1.8984375
- gate_weight: bfloat16 [2048, 5120], P('fs', 'tp'), may hold values from -0.125 to 0.125
- up_weight: bfloat16 [2048, 5120], P('fs', 'tp'), may hold values from -0.125 to 0.125
- down_weight: bfloat16 [5120, 2048], P('tp', 'fs'), may hold values from -0.078125 to 0.078125
Outputs:
- mixed: bfloat16 [32768, 2048], P(('grp', 'fs', 'tp')), parts along dimension 0
There are 2 independent parts, one for each index of `grp`. A program takes and returns all parts, laid end to end along the dimension named above; an argument that names none is the same for every part. Nothing has to cross between parts.
All inputs are finite; a program needn't handle non-finite values.
Results may differ from a plain program's by a relative error of at most 0.013.
Values may be sent and summed in bfloat16 or wider, within the bound.
No kernel may reach another device: no remote copies, remote signals or barrier semaphores. Data moves between devices by JAX's collectives and lax.ppermute only.
A program may use at most 64 MiB of HBM per device.

v0:
```python
import jax
import jax.numpy as jnp
from jax import lax
from jax.sharding import PartitionSpec as P

EPSILON = 1e-06


def side_by_side(arrays, axis, dim, along):
    widths = [a.shape[along] for a in arrays]
    both = jnp.concatenate(arrays, axis=along)
    result = lax.all_gather(both, axis, axis=dim, tiled=True)
    return tuple(jnp.split(result, [sum(widths[:k]) for k in range(1, len(widths))], axis=along))


def normalize(tokens, norm_gain):
    as_float = tokens.astype(jnp.float32)
    scale = lax.rsqrt(jnp.mean(as_float * as_float, axis=-1, keepdims=True) + EPSILON)
    return (as_float * scale * norm_gain.astype(jnp.float32)).astype(jnp.bfloat16)


def rounded(values):
    return lax.optimization_barrier(values.astype(jnp.bfloat16)).astype(jnp.float32)


def on_device(tokens, norm_gain, gate_weight, up_weight, down_weight):
    normed = normalize(tokens, norm_gain)
    down_whole = lax.all_gather(down_weight, "fs", axis=1, tiled=True)
    gate_whole, up_whole = side_by_side((gate_weight, up_weight), "fs", 0, 1)
    gate_acts = jnp.dot(normed, gate_whole, preferred_element_type=jnp.float32)
    up_acts = jnp.dot(normed, up_whole, preferred_element_type=jnp.float32)
    hidden = (jax.nn.silu(gate_acts) * up_acts).astype(jnp.bfloat16)
    return lax.psum_scatter(
        rounded(jnp.dot(hidden, down_whole, preferred_element_type=jnp.float32)).astype(
            jnp.bfloat16
        ),
        "tp",
        scatter_dimension=0,
        tiled=True,
    )


def solution(mesh):
    return jax.shard_map(
        on_device,
        mesh=mesh,
        in_specs=(P(("grp", "fs"), None), P(), P("fs", "tp"), P("fs", "tp"), P("tp", "fs")),
        out_specs=P(("grp", "fs", "tp"), None),
        check_vma=False,
    )
```

profile of v0, /device:TPU:40, one launch (start us, length us, event | category | flops | bytes accessed | tf_op | source)
XLA Modules:
  0.0 240.0 jit_solution(12156880815646767167)
XLA Ops:
  6.5 0.0 all-gather.3.cloned.1.call-start
  6.6 1.7 pad_maximum_fusion
  8.3 0.1 all-gather.3.cloned.1.call-update
  8.4 0.1 all-gather.5.cloned.1.call-start
  8.4 0.7 all-gather.5.cloned.1.call-update
  9.2 0.1 reduce-scatter.2.cloned.1.call-start
  9.2 0.7 convert_element_type.18
  9.9 3.1 %fusion = f32[1024]{0:T(1024)S(1)} fusion(bf16[1024,2048]{1,0:T(8,128)(2,1)} %param.5), kind=kLoop, calls=%fused_computation.2 | loop fusion | flops 6290432 | bytes 4198400 | tf_op jit(solution)/shard_map/reduce_sum | solution.py:18
  13.0 88.4 %all-gather.3.cloned.1.call-done = bf16[2048,1280]{1,0:T(8,128)(2,1)} async-done(((bf16[128,1280]{1,0:T(8,128)(2,1)}), bf16[2048,1280]{1,0:T(8,128)(2,1)}) %all-gather.3.cloned.1.call-update) | async-done | bytes 5242896 | tf_op jit(solution)/shard_map/all_gather | solution.py:12
  101.4 6.3 %fusion.3 = f32[1024,640]{1,0:T(8,128)S(1)} fusion(bf16[2048,1280]{1,0:T(8,128)(2,1)} %all-gather.3.cloned.1.call-done, bf16[1024,2048]{1,0:T(8,128)(2,1)} %param.5, f32[2048]{0:T(1024)S(1)} %convert_element_type.18, f32[1024]{0:T(1024)S(1)} %add_rsqrt_fusion), kind=kOutput, calls=%fused_computation.6 | convolution fusion | flops 2692743168 | bytes 9449472 | tf_op jit(solution)/shard_map/dot_general | solution.py:31
  107.7 72.3 %all-gather.5.cloned.1.call-done = bf16[640,2048]{1,0:T(8,128)(2,1)} async-done(((bf16[640,128]{1,0:T(8,128)(2,1)}), bf16[640,2048]{1,0:T(8,128)(2,1)}) %all-gather.5.cloned.1.call-update) | async-done | bytes 2621456 | tf_op jit(solution)/shard_map/all_gather | solution.py:28
  180.0 12.9 %convolution_convert_fusion = bf16[1024,2048]{1,0:T(8,128)(2,1)} fusion(bf16[640,2048]{1,0:T(8,128)(2,1)} %all-gather.5.cloned.1.call-done, f32[1024,640]{1,0:T(8,128)S(1)} %fusion.3, bf16[2048,1280]{1,0:T(8,128)(2,1)} %all-gather.3.cloned.1.call-done, bf16[1024,2048]{1,0:T(8,128)(2,1)} %param.5, f32[2048]{0:T(1024)S(1)} %convert_element_type.18, ...), kind=kOutput, calls=%fused_computation.5 | convolution fusion | flops 5383127040 | bytes 16265216 | tf_op jit(solution)/shard_map/dot_general | solution.py:34
  192.9 0.1 reduce-scatter.2.cloned.1.call-update
  192.9 40.5 %reduce-scatter.2.cloned.1.call-done = bf16[128,2048]{1,0:T(8,128)(2,1)} async-done(((bf16[1024,2048]{1,0:T(8,128)(2,1)}), bf16[128,2048]{1,0:T(8,128)(2,1)}) %reduce-scatter.2.cloned.1.call-update) | async-done | bytes 524304 | tf_op jit(solution)/shard_map/reduce_scatter | solution.py:33
  (1 shorter events, 0.0 us)
Async XLA Ops:
  6.5 94.9 %all-gather.3.cloned.1.call-start = ((), (), s32[]{:S(2)}) async-start(), calls=%async_computation.1 | async-start | bytes 5570560 | tf_op jit(solution)/shard_map/all_gather | solution.py:12
  8.4 171.7 %all-gather.5.cloned.1.call-start = ((), (), s32[]{:S(2)}) async-start(), calls=%async_computation.2 | async-start | bytes 2785280 | tf_op jit(solution)/shard_map/all_gather | solution.py:28
  9.2 224.2 %reduce-scatter.2.cloned.1.call-start = ((), (), s32[]{:S(2)}) async-start(), calls=%async_computation.3 | async-start | bytes 4718592 | tf_op jit(solution)/shard_map/reduce_scatter | solution.py:33
Sparse Core Ops, SparseCore 0:
  9.1 92.2 all-gather.2
  103.2 76.7 all-gather.4
  193.0 40.3 reduce-scatter.1
where the time goes:
time: 240 us
  waiting for transfers between devices  202 us (84%)
  matrix products  19.1 us (8%)
  between operations  13.1 us (5%)
  other arithmetic  5.51 us (2%)
    all_gather x1, waiting for transfers between devices, side_by_side(): result = lax.all_gather(both, axis, axis=dim, tiled=True)  88.4 us
    all_gather x1, waiting for transfers between devices, on_device(): down_whole = lax.all_gather(down_weight, 'fs', axis=1, tiled=True)  72.3 us
    reduce_scatter x1, waiting for transfers between devices, on_device(): lax.psum_scatter(rounded(jnp.dot(hidden, down_whole, preferred_element_ty...  40.5 us
    dot_general x1, matrix products, on_device(): jnp.dot(hidden, down_whole, preferred_element_type=jnp.float32)  12.9 us
    dot_general x1, matrix products, on_device(): up_acts = jnp.dot(normed, up_whole, preferred_element_type=jnp.float32)  6.29 us
  transfers between devices with their start and end apart: 3, of which 3 were waited for; matrix products, arithmetic and copies ran while one was open for 4% of the time, Pallas kernels for 0%

commit v1 on v0

--- a/solution.py
+++ b/solution.py
@@ -4,6 +4,19 @@
 from jax.sharding import PartitionSpec as P
 
 EPSILON = 1e-06
+
+
+def gather_around(value, axis, dim):
+    ways = lax.axis_size(axis)
+    up = [(d, (d + 1) % ways) for d in range(ways)]
+    down = [(d, (d - 1) % ways) for d in range(ways)]
+    earlier, later = ([value], [value])
+    for _ in range(ways // 2):
+        earlier.append(lax.ppermute(earlier[-1], axis, up))
+    for _ in range((ways - 1) // 2):
+        later.append(lax.ppermute(later[-1], axis, down))
+    line = jnp.concatenate([*earlier[::-1], *later[1:]], axis=dim)
+    return jnp.roll(line, (lax.axis_index(axis) - ways // 2) * value.shape[dim], axis=dim)
 
 
 def side_by_side(arrays, axis, dim, along):
@@ -25,7 +38,7 @@
 
 def on_device(tokens, norm_gain, gate_weight, up_weight, down_weight):
     normed = normalize(tokens, norm_gain)
-    down_whole = lax.all_gather(down_weight, "fs", axis=1, tiled=True)
+    down_whole = gather_around(down_weight, "fs", 1)
     gate_whole, up_whole = side_by_side((gate_weight, up_weight), "fs", 0, 1)
     gate_acts = jnp.dot(normed, gate_whole, preferred_element_type=jnp.float32)
     up_acts = jnp.dot(normed, up_whole, preferred_element_type=jnp.float32)

time: 240 us -> 196 us (0.82)
  waiting for transfers between devices: 202 us -> 105 us
  starting transfers between devices: 0.13 us -> 28.5 us
  local copies, waits for them, and re-layouts: 0 us -> 22.6 us
    all_gather x1, waiting for transfers between devices: 88.4 us -> 0.01 us  [side_by_side(): result = lax.all_gather(both, axis, axis=dim, tiled=True)]
    all_gather x1 -> x0, waiting for transfers between devices: 72.3 us -> none  [on_device(): down_whole = lax.all_gather(down_weight, 'fs', axis=1, tiled=True)]
    ppermute x0 -> x15, waiting for transfers between devices: none -> 66.6 us  [the longest x8 60.2 us: gather_around(): earlier.append(lax.ppermute(earlier[-1], axis, up))]
    ppermute x0 -> x15, starting transfers between devices: none -> 28.4 us  [the longest x7 24.8 us: gather_around(): later.append(lax.ppermute(later[-1], axis, down))]
    unnamed x0 -> x33, local copies, waits for them, and re-layouts: none -> 21.9 us
  transfers between devices with their start and end apart: 3 -> 17, of which waited for: 3 -> 14; matrix products, arithmetic and copies ran while one was open for 4% -> 13% of each run, Pallas kernels for 0% -> 0%
where the time goes in v1:
time: 196 us
  waiting for transfers between devices  105 us (54%)
  starting transfers between devices  28.5 us (15%)
  local copies, waits for them, and re-layouts  22.6 us (12%)
  matrix products  21.1 us (11%)
  between operations  13.5 us (7%)
  other arithmetic  5.58 us (3%)
    ppermute x8, waiting for transfers between devices, gather_around(): earlier.append(lax.ppermute(earlier[-1], axis, up))  60.2 us
    reduce_scatter x1, waiting for transfers between devices, on_device(): lax.psum_scatter(rounded(jnp.dot(hidden, down_whole, preferred_element_ty...  38.1 us
    ppermute x7, starting transfers between devices, gather_around(): later.append(lax.ppermute(later[-1], axis, down))  24.8 us
    unnamed x33, local copies, waits for them, and re-layouts  21.9 us
    dot_general x1, matrix products, on_device(): jnp.dot(hidden, down_whole, preferred_element_type=jnp.float32)  13.1 us
    dot_general x1, matrix products, on_device(): up_acts = jnp.dot(normed, up_whole, preferred_element_type=jnp.float32)  7.94 us
    ppermute x7, waiting for transfers between devices, gather_around(): later.append(lax.ppermute(later[-1], axis, down))  6.44 us
  transfers between devices with their start and end apart: 17, of which 14 were waited for; matrix products, arithmetic and copies ran while one was open for 13% of the time, Pallas kernels for 0%

profile of v1, /device:TPU:40, one launch (start us, length us, event | category | flops | bytes accessed | tf_op | source)
XLA Modules:
  0.0 196.1 jit_solution(2840100580070030740)
XLA Ops:
  6.6 1.8 pad_maximum_fusion
  8.3 0.1 all-gather.2.cloned.1.call-update
  8.4 0.1 reduce-scatter.2.cloned.1.call-start
  8.5 2.9 %collective-permute-start = (bf16[640,128]{1,0:T(8,128)(2,1)}, bf16[640,128]{1,0:T(8,128)(2,1)S(1)}, u32[]{:S(2)}, u32[]{:S(2)}) collective-permute-start(bf16[640,128]{1,0:T(8,128)(2,1)} %param.9), channel_id=1, source_target_pairs={{0,8},{8,16},{16,24},{24,32},{32,40},{40,48},{48,56},{56,64},{64,7... | collective-permute-start | bytes 491528 | tf_op jit(solution)/shard_map/ppermute | solution.py:15
  11.4 24.1 %collective-permute-done = bf16[640,128]{1,0:T(8,128)(2,1)S(1)} collective-permute-done((bf16[640,128]{1,0:T(8,128)(2,1)}, bf16[640,128]{1,0:T(8,128)(2,1)S(1)}, u32[]{:S(2)}, u32[]{:S(2)}) %collective-permute-start) | collective-permute-done | bytes 163872 | tf_op jit(solution)/shard_map/ppermute | solution.py:15
  35.5 3.2 %collective-permute-start.8 = (bf16[640,128]{1,0:T(8,128)(2,1)}, bf16[640,128]{1,0:T(8,128)(2,1)S(1)}, u32[]{:S(2)}, u32[]{:S(2)}) collective-permute-start(bf16[640,128]{1,0:T(8,128)(2,1)} %param.9), channel_id=1, source_target_pairs={{0,120},{8,0},{16,8},{24,16},{32,24},{40,32},{48,40},{56,48},{64,5... | collective-permute-start | bytes 491528 | tf_op jit(solution)/shard_map/ppermute | solution.py:17
  38.7 5.0 %collective-permute-done.1 = bf16[640,128]{1,0:T(8,128)(2,1)S(1)} collective-permute-done((bf16[640,128]{1,0:T(8,128)(2,1)S(1)}, bf16[640,128]{1,0:T(8,128)(2,1)S(1)}, u32[]{:S(2)}, u32[]{:S(2)}) %collective-permute-start.1) | collective-permute-done | bytes 163872 | tf_op jit(solution)/shard_map/ppermute | solution.py:15
  43.7 0.7 collective-permute-start.2
  44.4 0.6 collective-permute-done.8
  45.0 3.6 %collective-permute-start.9 = (bf16[640,128]{1,0:T(8,128)(2,1)S(1)}, bf16[640,128]{1,0:T(8,128)(2,1)S(1)}, u32[]{:S(2)}, u32[]{:S(2)}) collective-permute-start(bf16[640,128]{1,0:T(8,128)(2,1)S(1)} %collective-permute-done.8), channel_id=1, source_target_pairs={{0,120},{8,0},{16,8},{24,16},{32,24},{40,32},{48,40},{56,48},{64,5... | collective-permute-start | bytes 491528 | tf_op jit(solution)/shard_map/ppermute | solution.py:17
  48.6 5.6 %collective-permute-done.2 = bf16[640,128]{1,0:T(8,128)(2,1)S(1)} collective-permute-done((bf16[640,128]{1,0:T(8,128)(2,1)S(1)}, bf16[640,128]{1,0:T(8,128)(2,1)S(1)}, u32[]{:S(2)}, u32[]{:S(2)}) %collective-permute-start.2) | collective-permute-done | bytes 163872 | tf_op jit(solution)/shard_map/ppermute | solution.py:15
  54.2 1.1 collective-permute-done.9
  55.3 3.7 %collective-permute-start.10 = (bf16[640,128]{1,0:T(8,128)(2,1)S(1)}, bf16[640,128]{1,0:T(8,128)(2,1)S(1)}, u32[]{:S(2)}, u32[]{:S(2)}) collective-permute-start(bf16[640,128]{1,0:T(8,128)(2,1)S(1)} %collective-permute-done.9), channel_id=1, source_target_pairs={{0,120},{8,0},{16,8},{24,16},{32,24},{40,32},{48,40},{56,48},{64,5... | collective-permute-start | bytes 491528 | tf_op jit(solution)/shard_map/ppermute | solution.py:17
  59.0 5.7 %collective-permute-done.3 = bf16[640,128]{1,0:T(8,128)(2,1)S(1)} collective-permute-done((bf16[640,128]{1,0:T(8,128)(2,1)S(1)}, bf16[640,128]{1,0:T(8,128)(2,1)S(1)}, u32[]{:S(2)}, u32[]{:S(2)}) %collective-permute-start.3) | collective-permute-done | bytes 163872 | tf_op jit(solution)/shard_map/ppermute | solution.py:15
  64.6 1.0 collective-permute-done.10
  65.7 3.7 %collective-permute-start.11 = (bf16[640,128]{1,0:T(8,128)(2,1)S(1)}, bf16[640,128]{1,0:T(8,128)(2,1)S(1)}, u32[]{:S(2)}, u32[]{:S(2)}) collective-permute-start(bf16[640,128]{1,0:T(8,128)(2,1)S(1)} %collective-permute-done.10), channel_id=1, source_target_pairs={{0,120},{8,0},{16,8},{24,16},{32,24},{40,32},{48,40},{56,48},{64,5... | collective-permute-start | bytes 491528 | tf_op jit(solution)/shard_map/ppermute | solution.py:17
  69.3 5.9 %collective-permute-done.4 = bf16[640,128]{1,0:T(8,128)(2,1)S(1)} collective-permute-done((bf16[640,128]{1,0:T(8,128)(2,1)S(1)}, bf16[640,128]{1,0:T(8,128)(2,1)S(1)}, u32[]{:S(2)}, u32[]{:S(2)}) %collective-permute-start.4) | collective-permute-done | bytes 163872 | tf_op jit(solution)/shard_map/ppermute | solution.py:15
  75.3 0.5 collective-permute-done.11
  75.8 3.7 %collective-permute-start.12 = (bf16[640,128]{1,0:T(8,128)(2,1)S(1)}, bf16[640,128]{1,0:T(8,128)(2,1)S(1)}, u32[]{:S(2)}, u32[]{:S(2)}) collective-permute-start(bf16[640,128]{1,0:T(8,128)(2,1)S(1)} %collective-permute-done.11), channel_id=1, source_target_pairs={{0,120},{8,0},{16,8},{24,16},{32,24},{40,32},{48,40},{56,48},{64,5... | collective-permute-start | bytes 491528 | tf_op jit(solution)/shard_map/ppermute | solution.py:17
  79.5 6.7 %collective-permute-done.5 = bf16[640,128]{1,0:T(8,128)(2,1)S(1)} collective-permute-done((bf16[640,128]{1,0:T(8,128)(2,1)S(1)}, bf16[640,128]{1,0:T(8,128)(2,1)S(1)}, u32[]{:S(2)}, u32[]{:S(2)}) %collective-permute-start.5) | collective-permute-done | bytes 163872 | tf_op jit(solution)/shard_map/ppermute | solution.py:15
  86.2 3.1 %fusion = f32[1024]{0:T(1024)S(1)} fusion(bf16[1024,2048]{1,0:T(8,128)(2,1)} %param.5), kind=kLoop, calls=%fused_computation.2 | loop fusion | flops 6290432 | bytes 4198400 | tf_op jit(solution)/shard_map/reduce_sum | solution.py:31
  89.3 0.7 convert_element_type.18
  90.0 3.2 %collective-permute-start.13 = (bf16[640,128]{1,0:T(8,128)(2,1)S(1)}, bf16[640,128]{1,0:T(8,128)(2,1)S(1)}, u32[]{:S(2)}, u32[]{:S(2)}) collective-permute-start(bf16[640,128]{1,0:T(8,128)(2,1)S(1)} %collective-permute-done.12), channel_id=1, source_target_pairs={{0,120},{8,0},{16,8},{24,16},{32,24},{40,32},{48,40},{56,48},{64,5... | collective-permute-start | bytes 491528 | tf_op jit(solution)/shard_map/ppermute | solution.py:17
  93.3 4.2 %collective-permute-done.6 = bf16[640,128]{1,0:T(8,128)(2,1)S(1)} collective-permute-done((bf16[640,128]{1,0:T(8,128)(2,1)S(1)}, bf16[640,128]{1,0:T(8,128)(2,1)S(1)}, u32[]{:S(2)}, u32[]{:S(2)}) %collective-permute-start.6) | collective-permute-done | bytes 163872 | tf_op jit(solution)/shard_map/ppermute | solution.py:15
  97.5 0.0 collective-permute-start.7
  97.5 3.2 %collective-permute-done.13 = bf16[640,128]{1,0:T(8,128)(2,1)S(1)} collective-permute-done((bf16[640,128]{1,0:T(8,128)(2,1)S(1)}, bf16[640,128]{1,0:T(8,128)(2,1)S(1)}, u32[]{:S(2)}, u32[]{:S(2)}) %collective-permute-start.13) | collective-permute-done | bytes 163872 | tf_op jit(solution)/shard_map/ppermute | solution.py:17
  100.6 3.7 %collective-permute-start.14 = (bf16[640,128]{1,0:T(8,128)(2,1)S(1)}, bf16[640,128]{1,0:T(8,128)(2,1)S(1)}, u32[]{:S(2)}, u32[]{:S(2)}) collective-permute-start(bf16[640,128]{1,0:T(8,128)(2,1)S(1)} %collective-permute-done.13), channel_id=1, source_target_pairs={{0,120},{8,0},{16,8},{24,16},{32,24},{40,32},{48,40},{56,48},{64,5... | collective-permute-start | bytes 491528 | tf_op jit(solution)/shard_map/ppermute | solution.py:17
  104.3 3.0 %collective-permute-done.7 = bf16[640,128]{1,0:T(8,128)(2,1)S(1)} collective-permute-done((bf16[640,128]{1,0:T(8,128)(2,1)S(1)}, bf16[640,128]{1,0:T(8,128)(2,1)S(1)}, u32[]{:S(2)}, u32[]{:S(2)}) %collective-permute-start.7) | collective-permute-done | bytes 163872 | tf_op jit(solution)/shard_map/ppermute | solution.py:15
  107.3 0.7 constant_dynamic-update-slice_fusion.31
  108.0 0.7 constant_dynamic-update-slice_fusion.30
  108.8 0.7 constant_dynamic-update-slice_fusion.29
  109.5 0.7 constant_dynamic-update-slice_fusion.28
  110.2 0.7 constant_dynamic-update-slice_fusion.27
  110.9 0.7 constant_dynamic-update-slice_fusion.26
  111.6 0.7 constant_dynamic-update-slice_fusion.25
  112.3 0.7 constant_dynamic-update-slice_fusion.24
  113.0 0.7 constant_dynamic-update-slice_fusion.23
  113.7 0.7 constant_dynamic-update-slice_fusion.22
  114.4 0.7 constant_dynamic-update-slice_fusion.21
  115.1 0.7 constant_dynamic-update-slice_fusion.20
  115.9 0.7 constant_dynamic-update-slice_fusion.19
  116.6 0.7 constant_dynamic-update-slice_fusion.18
  117.3 0.7 constant_dynamic-update-slice_fusion.17
  118.0 0.7 constant_dynamic-update-slice_fusion.16
  118.7 0.7 constant_dynamic-update-slice_fusion.15
  119.3 0.7 constant_dynamic-update-slice_fusion.14
  120.0 0.7 constant_dynamic-update-slice_fusion.13
  120.7 0.7 constant_dynamic-update-slice_fusion.12
  121.4 0.7 constant_dynamic-update-slice_fusion.11
  122.1 0.7 constant_dynamic-update-slice_fusion.10
  122.8 0.7 constant_dynamic-update-slice_fusion.9
  123.6 0.7 constant_dynamic-update-slice_fusion.8
  124.3 0.7 constant_dynamic-update-slice_fusion.7
  125.0 0.7 constant_dynamic-update-slice_fusion.6
  125.7 0.8 constant_dynamic-update-slice_fusion.5
  126.4 0.7 constant_dynamic-update-slice_fusion.4
  127.2 0.7 constant_dynamic-update-slice_fusion.3
  127.8 0.7 constant_dynamic-update-slice_fusion.2
  128.5 0.7 constant_dynamic-update-slice_fusion.1
  129.3 0.8 constant_dynamic-update-slice_fusion
  130.0 7.9 %fusion.3 = f32[1024,640]{1,0:T(8,128)} fusion(bf16[2048,1280]{1,0:T(8,128)(2,1)} %all-gather.2.cloned.1.call-done, bf16[1024,2048]{1,0:T(8,128)(2,1)} %param.5, f32[2048]{0:T(1024)S(1)} %convert_element_type.18, f32[1024]{0:T(1024)S(1)} %add_rsqrt_fusion), kind=kOutput, calls=%fused_computation.6 | convolution fusion | flops 2692743168 | bytes 9449472 | tf_op jit(solution)/shard_map/dot_general | solution.py:44
  138.0 13.1 %convolution_convert_fusion = bf16[1024,2048]{1,0:T(8,128)(2,1)} fusion(bf16[640,4096]{1,0:T(8,128)(2,1)} %constant_dynamic-update-slice_fusion, s32[]{:T(128)S(6)} %select_n.14, f32[1024,640]{1,0:T(8,128)} %fusion.3, bf16[2048,1280]{1,0:T(8,128)(2,1)} %all-gather.2.cloned.1.call-done, bf16[1024,2048]{1,0:T(8,128)(2,1)} %param.5, ...), kind=kOutput, calls=%fused_computation.5 | convolution fusion | flops 5383127040 | bytes 16265220 | tf_op jit(solution)/shard_map/dot_general | solution.py:47
  151.1 0.1 reduce-scatter.2.cloned.1.call-update
  151.1 38.1 %reduce-scatter.2.cloned.1.call-done = bf16[128,2048]{1,0:T(8,128)(2,1)} async-done(((bf16[1024,2048]{1,0:T(8,128)(2,1)}), bf16[128,2048]{1,0:T(8,128)(2,1)}) %reduce-scatter.2.cloned.1.call-update) | async-done | bytes 524304 | tf_op jit(solution)/shard_map/reduce_scatter | solution.py:46
  (12 shorter events, 0.0 us)
Async XLA Ops:
  6.5 106.5 %copy-start = (bf16[640,128]{1,0:T(8,128)(2,1)S(1)}, bf16[640,128]{1,0:T(8,128)(2,1)}, u32[]{:S(2)}) copy-start(bf16[640,128]{1,0:T(8,128)(2,1)} %param.9) | copy-start | bytes 491524
  6.5 123.5 %all-gather.2.cloned.1.call-start = ((), (), s32[]{:S(2)}) async-start(), calls=%async_computation.1 | async-start | bytes 5570560 | tf_op jit(solution)/shard_map/all_gather | solution.py:25
  8.4 180.9 %reduce-scatter.2.cloned.1.call-start = ((), (), s32[]{:S(2)}) async-start(), calls=%async_computation.2 | async-start | bytes 4718592 | tf_op jit(solution)/shard_map/reduce_scatter | solution.py:46
  8.5 27.0 %collective-permute-start = (bf16[640,128]{1,0:T(8,128)(2,1)}, bf16[640,128]{1,0:T(8,128)(2,1)S(1)}, u32[]{:S(2)}, u32[]{:S(2)}) collective-permute-start(bf16[640,128]{1,0:T(8,128)(2,1)} %param.9), channel_id=1, source_target_pairs={{0,8},{8,16},{16,24},{24,32},{32,40},{40,48},{48,56},{56,64},{64,7... | collective-permute-start | bytes 491528 | tf_op jit(solution)/shard_map/ppermute | solution.py:15
  35.5 8.2 %collective-permute-start.1 = (bf16[640,128]{1,0:T(8,128)(2,1)S(1)}, bf16[640,128]{1,0:T(8,128)(2,1)S(1)}, u32[]{:S(2)}, u32[]{:S(2)}) collective-permute-start(bf16[640,128]{1,0:T(8,128)(2,1)S(1)} %collective-permute-done), channel_id=1, source_target_pairs={{0,8},{8,16},{16,24},{24,32},{32,40},{40,48},{48,56},{56,64},{64,7... | collective-permute-start | bytes 491528 | tf_op jit(solution)/shard_map/ppermute | solution.py:15
  35.5 9.5 %collective-permute-start.8 = (bf16[640,128]{1,0:T(8,128)(2,1)}, bf16[640,128]{1,0:T(8,128)(2,1)S(1)}, u32[]{:S(2)}, u32[]{:S(2)}) collective-permute-start(bf16[640,128]{1,0:T(8,128)(2,1)} %param.9), channel_id=1, source_target_pairs={{0,120},{8,0},{16,8},{24,16},{32,24},{40,32},{48,40},{56,48},{64,5... | collective-permute-start | bytes 491528 | tf_op jit(solution)/shard_map/ppermute | solution.py:17
  43.7 10.5 %collective-permute-start.2 = (bf16[640,128]{1,0:T(8,128)(2,1)S(1)}, bf16[640,128]{1,0:T(8,128)(2,1)S(1)}, u32[]{:S(2)}, u32[]{:S(2)}) collective-permute-start(bf16[640,128]{1,0:T(8,128)(2,1)S(1)} %collective-permute-done.1), channel_id=1, source_target_pairs={{0,8},{8,16},{16,24},{24,32},{32,40},{40,48},{48,56},{56,64},{64,7... | collective-permute-start | bytes 491528 | tf_op jit(solution)/shard_map/ppermute | solution.py:15
  45.0 10.3 %collective-permute-start.9 = (bf16[640,128]{1,0:T(8,128)(2,1)S(1)}, bf16[640,128]{1,0:T(8,128)(2,1)S(1)}, u32[]{:S(2)}, u32[]{:S(2)}) collective-permute-start(bf16[640,128]{1,0:T(8,128)(2,1)S(1)} %collective-permute-done.8), channel_id=1, source_target_pairs={{0,120},{8,0},{16,8},{24,16},{32,24},{40,32},{48,40},{56,48},{64,5... | collective-permute-start | bytes 491528 | tf_op jit(solution)/shard_map/ppermute | solution.py:17
  54.2 10.5 %collective-permute-start.3 = (bf16[640,128]{1,0:T(8,128)(2,1)S(1)}, bf16[640,128]{1,0:T(8,128)(2,1)S(1)}, u32[]{:S(2)}, u32[]{:S(2)}) collective-permute-start(bf16[640,128]{1,0:T(8,128)(2,1)S(1)} %collective-permute-done.2), channel_id=1, source_target_pairs={{0,8},{8,16},{16,24},{24,32},{32,40},{40,48},{48,56},{56,64},{64,7... | collective-permute-start | bytes 491528 | tf_op jit(solution)/shard_map/ppermute | solution.py:15
  55.3 10.4 %collective-permute-start.10 = (bf16[640,128]{1,0:T(8,128)(2,1)S(1)}, bf16[640,128]{1,0:T(8,128)(2,1)S(1)}, u32[]{:S(2)}, u32[]{:S(2)}) collective-permute-start(bf16[640,128]{1,0:T(8,128)(2,1)S(1)} %collective-permute-done.9), channel_id=1, source_target_pairs={{0,120},{8,0},{16,8},{24,16},{32,24},{40,32},{48,40},{56,48},{64,5... | collective-permute-start | bytes 491528 | tf_op jit(solution)/shard_map/ppermute | solution.py:17
  64.6 10.7 %collective-permute-start.4 = (bf16[640,128]{1,0:T(8,128)(2,1)S(1)}, bf16[640,128]{1,0:T(8,128)(2,1)S(1)}, u32[]{:S(2)}, u32[]{:S(2)}) collective-permute-start(bf16[640,128]{1,0:T(8,128)(2,1)S(1)} %collective-permute-done.3), channel_id=1, source_target_pairs={{0,8},{8,16},{16,24},{24,32},{32,40},{40,48},{48,56},{56,64},{64,7... | collective-permute-start | bytes 491528 | tf_op jit(solution)/shard_map/ppermute | solution.py:15
  65.7 10.2 %collective-permute-start.11 = (bf16[640,128]{1,0:T(8,128)(2,1)S(1)}, bf16[640,128]{1,0:T(8,128)(2,1)S(1)}, u32[]{:S(2)}, u32[]{:S(2)}) collective-permute-start(bf16[640,128]{1,0:T(8,128)(2,1)S(1)} %collective-permute-done.10), channel_id=1, source_target_pairs={{0,120},{8,0},{16,8},{24,16},{32,24},{40,32},{48,40},{56,48},{64,5... | collective-permute-start | bytes 491528 | tf_op jit(solution)/shard_map/ppermute | solution.py:17
  75.3 10.9 %collective-permute-start.5 = (bf16[640,128]{1,0:T(8,128)(2,1)S(1)}, bf16[640,128]{1,0:T(8,128)(2,1)S(1)}, u32[]{:S(2)}, u32[]{:S(2)}) collective-permute-start(bf16[640,128]{1,0:T(8,128)(2,1)S(1)} %collective-permute-done.4), channel_id=1, source_target_pairs={{0,8},{8,16},{16,24},{24,32},{32,40},{40,48},{48,56},{56,64},{64,7... | collective-permute-start | bytes 491528 | tf_op jit(solution)/shard_map/ppermute | solution.py:15
  75.8 14.2 %collective-permute-start.12 = (bf16[640,128]{1,0:T(8,128)(2,1)S(1)}, bf16[640,128]{1,0:T(8,128)(2,1)S(1)}, u32[]{:S(2)}, u32[]{:S(2)}) collective-permute-start(bf16[640,128]{1,0:T(8,128)(2,1)S(1)} %collective-permute-done.11), channel_id=1, source_target_pairs={{0,120},{8,0},{16,8},{24,16},{32,24},{40,32},{48,40},{56,48},{64,5... | collective-permute-start | bytes 491528 | tf_op jit(solution)/shard_map/ppermute | solution.py:17
  86.2 11.2 %collective-permute-start.6 = (bf16[640,128]{1,0:T(8,128)(2,1)S(1)}, bf16[640,128]{1,0:T(8,128)(2,1)S(1)}, u32[]{:S(2)}, u32[]{:S(2)}) collective-permute-start(bf16[640,128]{1,0:T(8,128)(2,1)S(1)} %collective-permute-done.5), channel_id=1, source_target_pairs={{0,8},{8,16},{16,24},{24,32},{32,40},{40,48},{48,56},{56,64},{64,7... | collective-permute-start | bytes 491528 | tf_op jit(solution)/shard_map/ppermute | solution.py:15
  90.0 10.6 %collective-permute-start.13 = (bf16[640,128]{1,0:T(8,128)(2,1)S(1)}, bf16[640,128]{1,0:T(8,128)(2,1)S(1)}, u32[]{:S(2)}, u32[]{:S(2)}) collective-permute-start(bf16[640,128]{1,0:T(8,128)(2,1)S(1)} %collective-permute-done.12), channel_id=1, source_target_pairs={{0,120},{8,0},{16,8},{24,16},{32,24},{40,32},{48,40},{56,48},{64,5... | collective-permute-start | bytes 491528 | tf_op jit(solution)/shard_map/ppermute | solution.py:17
  97.5 9.9 %collective-permute-start.7 = (bf16[640,128]{1,0:T(8,128)(2,1)S(1)}, bf16[640,128]{1,0:T(8,128)(2,1)S(1)}, u32[]{:S(2)}, u32[]{:S(2)}) collective-permute-start(bf16[640,128]{1,0:T(8,128)(2,1)S(1)} %collective-permute-done.6), channel_id=1, source_target_pairs={{0,8},{8,16},{16,24},{24,32},{32,40},{40,48},{48,56},{56,64},{64,7... | collective-permute-start | bytes 491528 | tf_op jit(solution)/shard_map/ppermute | solution.py:15
  100.6 17.3 %collective-permute-start.14 = (bf16[640,128]{1,0:T(8,128)(2,1)S(1)}, bf16[640,128]{1,0:T(8,128)(2,1)S(1)}, u32[]{:S(2)}, u32[]{:S(2)}) collective-permute-start(bf16[640,128]{1,0:T(8,128)(2,1)S(1)} %collective-permute-done.13), channel_id=1, source_target_pairs={{0,120},{8,0},{16,8},{24,16},{32,24},{40,32},{48,40},{56,48},{64,5... | collective-permute-start | bytes 491528 | tf_op jit(solution)/shard_map/ppermute | solution.py:17
Sparse Core Ops, SparseCore 0:
  9.1 108.8 all-gather.1
  151.3 37.9 reduce-scatter.1
